TPU v7x, 32 devices: a whole 2x2x4 slice. The times are simulated.
32 devices in a mesh: sp: 8 (over z, x), tp: 4 (over y, core).
Axes of the slice: x: 2, y: 2, z: 4, core: 2. Of those that a mesh axis runs over, the one named last changes fastest.
Arguments:
- layer_input: bfloat16 [8, 1536, 2048], P('sp', 'tp'), may hold values from -6 to 6
- input_gain: float32 [2048], replicated, may hold values from 0.1 to 1.9
- key_weight: bfloat16 [2048, 512], P('sp', 'tp'), may hold values from -0.125 to 0.125
- value_weight: bfloat16 [2048, 512], P('sp', 'tp'), may hold values from -0.125 to 0.125
- key_gain: float32 [128], replicated, may hold values from 0.1 to 1.9
- stop_shift: bfloat16 [8, 4, 1536], P('sp', None, 'tp'), may hold values from -20 to 0
- new_query: bfloat16 [8, 16, 128], P('sp', 'tp'), may hold values from -6 to 6
- query_gain: float32 [128], replicated, may hold values from 0.1 to 1.9
- out_gain: float32 [128], replicated, may hold values from 0.1 to 1.9
Outputs:
- key_cache: bfloat16 [8, 4, 1536, 128], P('sp', 'tp')
- value_cache: bfloat16 [8, 4, 1536, 128], P('sp', 'tp')
- shift_cache: bfloat16 [8, 4, 1536], P('sp', 'tp')
- first_read: bfloat16 [8, 16, 128], P('sp', 'tp')
All inputs are finite; a program needn't handle non-finite values.
Results may differ from a plain program's by a relative error of at most 0.013.
Values may be sent and summed in bfloat16 or wider, within the bound.
A program may use at most 64 MiB of HBM per device.

v0:
```python
import jax
import jax.numpy as jnp
from jax import lax
from jax.sharding import PartitionSpec as P

KVH = 4


epsilon = 1e-06


def row_norm(value_entries, scaling):
    return (
        value_entries
        * lax.rsqrt(jnp.mean(value_entries * value_entries, axis=-1, keepdims=True) + epsilon)
        * scaling
    )


def shards(
    layer_input,
    input_gain,
    key_weight,
    value_weight,
    key_gain,
    stop_shift,
    new_query,
    query_gain,
    out_gain,
):
    groups = lax.axis_size("tp")
    copies = groups // KVH
    row_count = layer_input.shape[1]
    head_size = new_query.shape[2]
    score_scale = 1.0 / head_size**0.5
    normed = row_norm(layer_input[0].astype(jnp.float32), input_gain).astype(jnp.bfloat16)
    stacked = jnp.stack((key_weight, value_weight), 0)
    full_depth = lax.all_gather(stacked, "sp", axis=1, tiled=True)
    projected = jnp.einsum(
        "rd,kdc->krc",
        normed,
        lax.all_gather(full_depth, "tp", axis=2, tiled=True),
        preferred_element_type=jnp.float32,
    )
    key_rows = row_norm(projected[0].reshape(row_count, KVH, head_size), key_gain).astype(
        jnp.bfloat16
    )
    value_rows = projected[1].reshape(row_count, KVH, head_size).astype(jnp.bfloat16)
    local_shift = stop_shift[0]
    key_slots = jnp.repeat(key_rows, copies, axis=1)
    value_slots = jnp.repeat(value_rows, copies, axis=1)
    shift_slots = jnp.repeat(local_shift.T, copies, axis=1)
    key_got, value_got, shift_got = (
        lax.all_to_all(key_slots, "tp", split_axis=1, concat_axis=0, tiled=True),
        lax.all_to_all(value_slots, "tp", split_axis=1, concat_axis=0, tiled=True),
        lax.all_to_all(shift_slots, "tp", split_axis=1, concat_axis=0, tiled=True),
    )
    key_line = key_got[:, 0, :]
    value_line = value_got[:, 0, :]
    shift_line = shift_got[:, 0]
    length = key_line.shape[0]
    query_rows = row_norm(new_query[0].astype(jnp.float32), query_gain).astype(jnp.bfloat16)
    scores = (
        jnp.einsum("qd,ld->ql", query_rows, key_line, preferred_element_type=jnp.float32)
        * score_scale
    )
    scores = scores + shift_line.astype(jnp.float32)[None, :]
    log_keep = jax.nn.log_sigmoid(-scores)
    inside = lax.cumsum(log_keep, axis=1, reverse=True) - log_keep
    weights = jnp.exp(jax.nn.log_sigmoid(scores) + inside).astype(jnp.bfloat16)
    read_sum = jnp.dot(weights, value_line, preferred_element_type=jnp.float32)
    first_out = row_norm(read_sum, out_gain).astype(jnp.bfloat16)
    return (
        key_line.reshape(1, 1, length, head_size),
        value_line.reshape(1, 1, length, head_size),
        shift_line.reshape(1, 1, length),
        first_out[None],
    )


def solution(mesh):
    placed = (
        P("sp", "tp", None),
        P(),
        P("sp", "tp"),
        P("sp", "tp"),
        P(),
        P("sp", None, "tp"),
        P("sp", "tp", None),
        P(),
        P(),
    )
    return jax.shard_map(
        shards,
        mesh=mesh,
        in_specs=placed,
        out_specs=(
            P("sp", "tp", None, None),
            P("sp", "tp", None, None),
            P("sp", "tp", None),
            P("sp", "tp", None),
        ),
        check_vma=False,
    )
```

profile of v0, /device:TPU:0, one launch (start us, length us, event | category | flops | bytes accessed | tf_op | source)
XLA Modules:
  0.0 125.1 jit_solution(7521093562815016131)
XLA Ops:
  7.2 1.0 copy.25
  8.3 0.9 copy.26
  9.2 0.7 pad_maximum_fusion
  10.0 42.8 %all-gather.3.cloned.1.call-done = bf16[2,2048,128]{1,2,0:T(8,128)(2,1)} async-done(((bf16[2,256,128]{1,2,0:T(8,128)(2,1)}), bf16[2,2048,128]{1,2,0:T(8,128)(2,1)}) %all-gather.3.cloned.1.call-update) | async-done | bytes 1048592 | tf_op jit(solution)/shard_map/all_gather | solution.py:38
  52.8 0.7 copy.36
  53.5 0.5 broadcast.75
  54.0 0.7 reduce.5
  54.7 0.7 reshape.96
  55.3 3.2 %all-to-all-start.2 = ((bf16[4,2,192]{2,1,0:T(2,128)(2,1)}), bf16[4,2,192]{2,1,0:T(2,128)(2,1)S(1)}, u32[]{:S(2)}, u32[]{:S(2)}) async-start(bf16[4,2,192]{2,1,0:T(2,128)(2,1)} %reshape.96), calls=%async_computation.2 | async-start | bytes 8192 | tf_op jit(solution)/shard_map/all_to_all | solution.py:56
  58.6 0.8 fusion.22
  59.4 1.9 %fusion = f32[384]{0:T(512)S(1)} fusion(bf16[1,384,2048]{2,1,0:T(8,128)(2,1)} %param.9), kind=kLoop, calls=%fused_computation.2 | loop fusion | flops 2358912 | bytes 1574400 | tf_op jit(solution)/shard_map/reduce_sum | solution.py:15
  61.4 26.5 %all-gather.5.cloned.1.call-done = bf16[2,2048,512]{1,2,0:T(8,128)(2,1)} async-done(((bf16[2,2048,128]{1,2,0:T(8,128)(2,1)}), bf16[2,2048,512]{1,2,0:T(8,128)(2,1)}) %all-gather.5.cloned.1.call-update) | async-done | bytes 4194320 | tf_op jit(solution)/shard_map/all_gather | solution.py:42
  87.8 4.6 %fusion.10 = f32[2,384,512]{1,2,0:T(8,128)S(1)} fusion(bf16[2,2048,512]{1,2,0:T(8,128)(2,1)} %all-gather.5.cloned.1.call-done, bf16[1,384,2048]{2,1,0:T(8,128)(2,1)S(1)} %copy-done, f32[2048]{0:T(1024)S(1)} %copy-done.6, f32[384]{0:T(512)S(1)} %add_rsqrt_fusion.1), kind=kOutput, calls=%fused_computation.12 | convolution fusion | flops 1613758464 | bytes 7349760 | tf_op jit(solution)/shard_map/rd,kdc->krc/dot_general | solution.py:39
  93.1 1.0 multiply_convert_fusion
  94.1 3.5 %all-to-all-start = ((bf16[384,4,128]{2,0,1:T(8,128)(2,1)}), bf16[384,4,128]{2,0,1:T(8,128)(2,1)S(1)}, u32[]{:S(2)}, u32[]{:S(2)}) async-start(bf16[384,4,128]{2,0,1:T(8,128)(2,1)} %multiply_convert_fusion), calls=%async_computation | async-start | bytes 786432 | tf_op jit(solution)/shard_map/all_to_all | solution.py:54
  97.8 0.9 copy.28
  98.7 6.3 %all-to-all-done = bf16[384,4,128]{2,0,1:T(8,128)(2,1)S(1)} async-done(((bf16[384,4,128]{2,0,1:T(8,128)(2,1)}), bf16[384,4,128]{2,0,1:T(8,128)(2,1)S(1)}, u32[]{:S(2)}, u32[]{:S(2)}) %all-to-all-start) | async-done | bytes 393248 | tf_op jit(solution)/shard_map/all_to_all | solution.py:54
  105.0 3.5 %all-to-all-start.1 = ((bf16[384,4,128]{2,0,1:T(8,128)(2,1)}), bf16[384,4,128]{2,0,1:T(8,128)(2,1)S(1)}, u32[]{:S(2)}, u32[]{:S(2)}) async-start(bf16[384,4,128]{2,0,1:T(8,128)(2,1)} %copy.28), calls=%async_computation.1 | async-start | bytes 786432 | tf_op jit(solution)/shard_map/all_to_all | solution.py:55
  108.8 5.0 %reduce-window.6 = f32[4,12,128]{2,1,0:T(8,128)S(1)} reduce-window(f32[4,12,128]{2,1,0:T(8,128)S(1)} %reshape.89, f32[]{:T(128)} %constant.8.clone.1), window={size=1x1x128 pad=0_0x0_0x0_127}, to_apply=%region_3.4 | reduce-window | flops 780288 | bytes 49156 | tf_op jit(solution)/shard_map/reduce-window
  114.2 1.6 %all-to-all-done.1 = bf16[384,4,128]{2,0,1:T(8,128)(2,1)S(1)} async-done(((bf16[384,4,128]{2,0,1:T(8,128)(2,1)}), bf16[384,4,128]{2,0,1:T(8,128)(2,1)S(1)}, u32[]{:S(2)}, u32[]{:S(2)}) %all-to-all-start.1) | async-done | bytes 393248 | tf_op jit(solution)/shard_map/all_to_all | solution.py:55
  115.8 0.3 multiply_reduce_fusion.1
  116.2 0.6 fusion.25
  116.8 0.7 copy.39
  117.5 0.7 copy.40
  (36 shorter events, 1.6 us)
Async XLA Ops:
  7.2 80.7 %copy-start = (bf16[1,384,2048]{2,1,0:T(8,128)(2,1)S(1)}, bf16[1,384,2048]{2,1,0:T(8,128)(2,1)}, u32[]{:S(2)}) copy-start(bf16[1,384,2048]{2,1,0:T(8,128)(2,1)} %param.9) | copy-start | bytes 4718596
  7.2 80.7 %copy-start.6 = (f32[2048]{0:T(1024)S(1)}, f32[2048]{0:T(1024)}, u32[]{:S(2)}) copy-start(f32[2048]{0:T(1024)} %param.10) | copy-start | bytes 24580
  7.2 45.6 %all-gather.3.cloned.1.call-start = ((), (), s32[]{:S(2)}) async-start(), calls=%async_computation.3 | async-start | bytes 1179648 | tf_op jit(solution)/shard_map/all_gather | solution.py:38
  9.9 77.9 %all-gather.5.cloned.1.call-start = ((), (), s32[]{:S(2)}) async-start(), calls=%async_computation.4 | async-start | bytes 5242880 | tf_op jit(solution)/shard_map/all_gather | solution.py:42
  55.3 38.8 %all-to-all-start.2 = ((bf16[4,2,192]{2,1,0:T(2,128)(2,1)}), bf16[4,2,192]{2,1,0:T(2,128)(2,1)S(1)}, u32[]{:S(2)}, u32[]{:S(2)}) async-start(bf16[4,2,192]{2,1,0:T(2,128)(2,1)} %reshape.96), calls=%async_computation.2 | async-start | bytes 8192 | tf_op jit(solution)/shard_map/all_to_all | solution.py:56
  92.5 0.7 copy-start.3
  92.5 15.9 %copy-start.2 = (bf16[1,4,128]{2,1,0:T(4,128)(2,1)S(1)}, bf16[1,4,128]{2,1,0:T(4,128)(2,1)}, u32[]{:S(2)}) copy-start(bf16[1,4,128]{2,1,0:T(4,128)(2,1)} %param.15) | copy-start | bytes 3076
  92.5 15.9 %copy-start.4 = (f32[128]{0:T(128)S(1)}, f32[128]{0:T(128)}, u32[]{:S(2)}) copy-start(f32[128]{0:T(128)} %param.16) | copy-start | bytes 1540
  92.8 23.3 %copy-start.5 = (f32[128]{0:T(128)S(1)}, f32[128]{0:T(128)}, u32[]{:S(2)}) copy-start(f32[128]{0:T(128)} %param.17) | copy-start | bytes 1540
  94.1 10.8 %all-to-all-start = ((bf16[384,4,128]{2,0,1:T(8,128)(2,1)}), bf16[384,4,128]{2,0,1:T(8,128)(2,1)S(1)}, u32[]{:S(2)}, u32[]{:S(2)}) async-start(bf16[384,4,128]{2,0,1:T(8,128)(2,1)} %multiply_convert_fusion), calls=%async_computation | async-start | bytes 786432 | tf_op jit(solution)/shard_map/all_to_all | solution.py:54
  97.7 20.6 %copy-start.1 = (bf16[4,1,384]{2,1,0:T(2,128)(2,1)}, bf16[4,1,384]{2,1,0:T(2,128)(2,1)S(1)}, u32[]{:S(2)}) copy-start(bf16[4,1,384]{2,1,0:T(2,128)(2,1)S(1)} %reshape.97) | copy-start | bytes 9220
  105.0 10.8 %all-to-all-start.1 = ((bf16[384,4,128]{2,0,1:T(8,128)(2,1)}), bf16[384,4,128]{2,0,1:T(8,128)(2,1)S(1)}, u32[]{:S(2)}, u32[]{:S(2)}) async-start(bf16[384,4,128]{2,0,1:T(8,128)(2,1)} %copy.28), calls=%async_computation.1 | async-start | bytes 786432 | tf_op jit(solution)/shard_map/all_to_all | solution.py:55
Sparse Core Ops, SparseCore 0:
  10.6 42.1 all-gather.2
  54.3 33.4 all-gather.4
where the time goes:
time: 126 us; the launch traced here: 125 us
  waiting for transfers between devices  77.2 us (61%)
  between operations  14.2 us (11%)
  other arithmetic  11.1 us (9%)
  starting transfers between devices  10.2 us (8%)
  local copies, waits for them, and re-layouts  7.15 us (6%)
  matrix products  5.2 us (4%)
    all_gather x1, waiting for transfers between devices, shards(): full_depth = lax.all_gather(stacked, 'sp', axis=1, tiled=True)  42.8 us
    all_gather x1, waiting for transfers between devices, shards(): lax.all_gather(full_depth, 'tp', axis=2, tiled=True)  26.5 us
    all_to_all x1, waiting for transfers between devices, shards(): lax.all_to_all(key_slots, 'tp', split_axis=1, concat_axis=0, tiled=True)  6.25 us
    another operation x2, other arithmetic  5.17 us
    unnamed x21, local copies, waits for them, and re-layouts  4.98 us
    dot_general x1, matrix products, shards(): jnp.einsum('rd,kdc->krc', normed, lax.all_gather(full_depth, 'tp', axis=2...  4.62 us
    all_to_all x1, starting transfers between devices, shards(): lax.all_to_all(key_slots, 'tp', split_axis=1, concat_axis=0, tiled=True)  3.46 us
    all_to_all x1, starting transfers between devices, shards(): lax.all_to_all(value_slots, 'tp', split_axis=1, concat_axis=0, tiled=True)  3.46 us
  transfers between devices with their start and end apart: 5, of which 4 were waited for; matrix products, arithmetic and copies ran while one was open for 14% of the time, Pallas kernels for 0%

commit v1 on v0

--- a/solution.py
+++ b/solution.py
@@ -1,6 +1,10 @@
+import functools
+
 import jax
 import jax.numpy as jnp
 from jax import lax
+from jax.experimental import pallas as pl
+from jax.experimental.pallas import tpu as pltpu
 from jax.sharding import PartitionSpec as P
 
 KVH = 4
@@ -77,8 +81,356 @@
         first_out[None],
     )
 
+CORES = 2
+PASS_LAST = 64
+
+
+def rms(entries):
+    return lax.rsqrt(jnp.mean(entries * entries, axis=-1, keepdims=True) + epsilon)
+
+
+def fused(
+    nx,
+    nz,
+    x_ref,
+    gain_ref,
+    kw_ref,
+    vw_ref,
+    key_gain_ref,
+    shift_ref,
+    query_ref,
+    query_gain_ref,
+    out_gain_ref,
+    key_out,
+    value_out,
+    shift_out,
+    read_out,
+    x_buf,
+    n_buf,
+    w_buf,
+    k_send,
+    v_send,
+    k_line,
+    v_line,
+    shift_buf,
+    local_sem,
+    out_sem,
+    act_sem,
+    shift_sem,
+    za_sem,
+    ya_sem,
+    xa_sem,
+    yb_sem,
+    xb_sem,
+    zb_sem,
+    kv_sem,
+):
+    sp, tp = lax.axis_index("sp"), lax.axis_index("tp")
+    z, x = sp // nx, sp % nx
+    y, core = tp // CORES, tp % CORES
+    rows = x_ref.shape[1]
+    depth, head = kw_ref.shape
+    width = gain_ref.shape[1]
+    cut = depth - PASS_LAST
+    far_y = 1 - y
+
+    def device(zz, xx, yy, cc):
+        return (zz * nx + xx, yy * CORES + cc)
+
+    def zs(d):
+        return lax.rem(z + d, nz)
+
+    partner = device(z, x, y, 1 - core)
+    y_peer = device(z, x, far_y, core)
+    x_peer = device(z, 1 - x, y, core)
+    z_peers = [device(zs(d), x, y, core) for d in range(1, nz)]
+    cross = device(z, x, far_y, 1 - core)
+
+    own = pl.multiple_of(sp * depth, depth)
+    locals_ = [
+        pltpu.make_async_copy(
+            kw_ref, w_buf.at[y, pl.ds(own, depth), pl.ds(0, head)], local_sem.at[0]
+        ),
+        pltpu.make_async_copy(
+            vw_ref, w_buf.at[y, pl.ds(own, depth), pl.ds(head, head)], local_sem.at[1]
+        ),
+        pltpu.make_async_copy(
+            x_ref.at[0], x_buf.at[core], local_sem.at[2]
+        ),
+    ]
+    for c in locals_:
+        c.start()
+
+    barrier = pltpu.get_barrier_semaphore()
+    greeted = [partner, y_peer, x_peer, cross] + z_peers
+    for peer in greeted:
+        pl.semaphore_signal(
+            barrier, inc=1, device_id=peer, device_id_type=pl.DeviceIdType.MESH
+        )
+    pl.semaphore_wait(barrier, len(greeted))
+
+    started = []
+
+    def send(src, dst, sems, index, peer):
+        c = pltpu.make_async_remote_copy(
+            src_ref=src,
+            dst_ref=dst,
+            send_sem=sems.at[0, index],
+            recv_sem=sems.at[1, index],
+            device_id=peer,
+            device_id_type=pl.DeviceIdType.MESH,
+        )
+        c.start()
+        started.append(c)
+        return c
+
+    def arrived(dst, sems, index, peer):
+        pltpu.make_async_remote_copy(
+            src_ref=dst,
+            dst_ref=dst,
+            send_sem=sems.at[0, index],
+            recv_sem=sems.at[1, index],
+            device_id=peer,
+            device_id_type=pl.DeviceIdType.MESH,
+        ).wait_recv()
+
+    def part_a(zz, xx, yy):
+        at = pl.multiple_of((zz * nx + xx) * depth, depth)
+        return w_buf.at[yy, pl.ds(at, cut), :]
+
+    def part_b(zz, xx, yy):
+        at = pl.multiple_of((zz * nx + xx) * depth + cut, PASS_LAST)
+        return w_buf.at[yy, pl.ds(at, PASS_LAST), :]
+
+    def send_part(part, sems, index, peer):
+        send(part, part, sems, index, peer)
+
+    locals_[0].wait()
+    locals_[1].wait()
+    b_own, a_own = part_b(z, x, y), part_a(z, x, y)
+    send_part(b_own, yb_sem, 0, y_peer)
+    send_part(b_own, xb_sem, 0, x_peer)
+    send_part(a_own, ya_sem, 0, y_peer)
+    send_part(a_own, xa_sem, 0, x_peer)
+    for d in range(1, nz):
+        send_part(a_own, za_sem, d - 1, z_peers[d - 1])
+    for d in range(1, nz):
+        send_part(b_own, zb_sem, d - 1, z_peers[d - 1])
+    act = send(x_ref.at[0], x_buf.at[core], act_sem, 0, partner)
+    for i, peer in enumerate((partner, y_peer, cross)):
+        send(shift_ref.at[0], shift_buf.at[tp], shift_sem, i, peer)
+
+    def normalise(which):
+        tile = 16
+
+        def body(i, _):
+            at = pl.multiple_of(i * tile, tile)
+            v = x_buf[which, pl.ds(at, tile), :].astype(jnp.float32)
+            n_buf[which, pl.ds(at, tile), :] = (v * rms(v) * gain_ref[...]).astype(jnp.bfloat16)
+            return 0
+
+        lax.fori_loop(0, rows // tile, body, 0, unroll=2)
+
+    locals_[2].wait()
+    normalise(core)
+
+    arrived(part_b(z, x, far_y), yb_sem, 0, y_peer)
+    send_part(part_b(z, x, far_y), xb_sem, 1, x_peer)
+    for d in range(1, nz):
+        send_part(part_b(z, x, far_y), zb_sem, (nz - 1) + d - 1, z_peers[d - 1])
+    arrived(part_b(z, 1 - x, y), xb_sem, 0, x_peer)
+    for d in range(1, nz):
+        send_part(part_b(z, 1 - x, y), zb_sem, 2 * (nz - 1) + d - 1, z_peers[d - 1])
+    arrived(part_a(z, x, far_y), ya_sem, 0, y_peer)
+    send_part(part_a(z, x, far_y), xa_sem, nz, x_peer)
+    for d in range(1, nz):
+        arrived(part_a(zs(nz - d), x, y), za_sem, d - 1, z_peers[nz - d - 1])
+        send_part(part_a(zs(nz - d), x, y), ya_sem, d, y_peer)
+        if d == 1:
+            send_part(part_a(zs(nz - d), x, y), xa_sem, d, x_peer)
+    arrived(part_b(z, 1 - x, far_y), xb_sem, 1, x_peer)
+    for d in range(1, nz):
+        send_part(part_b(z, 1 - x, far_y), zb_sem, 3 * (nz - 1) + d - 1, z_peers[d - 1])
+    for d in range(1, nz):
+        arrived(part_a(zs(nz - d), x, far_y), ya_sem, d, y_peer)
+        send_part(part_a(zs(nz - d), x, far_y), xa_sem, nz + d, x_peer)
+    for d in range(2, nz):
+        send_part(part_a(zs(nz - d), x, y), xa_sem, d, x_peer)
+
+    arrived(x_buf.at[1 - core], act_sem, 0, partner)
+    normalise(1 - core)
+
+    def project(which, yy):
+        raw = jnp.dot(n_buf[which], w_buf[yy], preferred_element_type=jnp.float32)
+        keys = raw[:, :head]
+        keys = keys * rms(keys) * key_gain_ref[...]
+        return keys.astype(jnp.bfloat16), raw[:, head:].astype(jnp.bfloat16)
+
+    for d in range(nz):
+        arrived(part_a(zs(nz - d) if d else z, 1 - x, far_y), xa_sem, nz + d, x_peer)
+    for g, (xx, yy) in ((1, (x, far_y)), (3, (1 - x, far_y))):
+        for d in range(1, nz):
+            arrived(
+                part_b(zs(nz - d), xx, yy), zb_sem, g * (nz - 1) + d - 1, z_peers[nz - d - 1]
+            )
+    base = y * CORES * rows
+    far_base = far_y * CORES * rows
+    for c in range(CORES):
+        keys, values = project(c, far_y)
+        k_send[c], v_send[c] = keys, values
+        at = pl.multiple_of(base + c * rows, rows)
+        send(k_send.at[c], k_line.at[pl.ds(at, rows), :], kv_sem, 2 * c, y_peer)
+        send(v_send.at[c], v_line.at[pl.ds(at, rows), :], kv_sem, 2 * c + 1, y_peer)
+
+    arrived(part_a(z, 1 - x, y), xa_sem, 0, x_peer)
+    for d in range(1, nz):
+        arrived(part_a(zs(nz - d), 1 - x, y), xa_sem, d, x_peer)
+    for g, (xx, yy) in ((0, (x, y)), (2, (1 - x, y))):
+        for d in range(1, nz):
+            arrived(
+                part_b(zs(nz - d), xx, yy), zb_sem, g * (nz - 1) + d - 1, z_peers[nz - d - 1]
+            )
+    for c in range(CORES):
+        keys, values = project(c, y)
+        at = pl.multiple_of(base + c * rows, rows)
+        k_line[pl.ds(at, rows), :] = keys
+        v_line[pl.ds(at, rows), :] = values
+
+    shift_buf[tp] = shift_ref[0]
+    arrived(shift_buf.at[y * CORES + 1 - core], shift_sem, 0, partner)
+    arrived(shift_buf.at[far_y * CORES + core], shift_sem, 1, y_peer)
+    arrived(shift_buf.at[far_y * CORES + 1 - core], shift_sem, 2, cross)
+    tps = shift_buf.shape[0]
+    pieces = []
+    for t in range(tps):
+        block = shift_buf[t].astype(jnp.float32)
+        mine = lax.broadcasted_iota(jnp.int32, block.shape, 0) == tp
+        pieces.append(jnp.sum(jnp.where(mine, block, 0.0), axis=0, keepdims=True))
+    shifts = jnp.concatenate(pieces, axis=1)
+    shift_out[0] = shifts.astype(jnp.bfloat16)
+
+    for c in range(CORES):
+        at = pl.multiple_of(far_base + c * rows, rows)
+        arrived(k_line.at[pl.ds(at, rows), :], kv_sem, 2 * c, y_peer)
+        arrived(v_line.at[pl.ds(at, rows), :], kv_sem, 2 * c + 1, y_peer)
+    outs = [
+        pltpu.make_async_copy(k_line, key_out.at[0, 0], out_sem.at[0]),
+        pltpu.make_async_copy(v_line, value_out.at[0, 0], out_sem.at[1]),
+    ]
+    for c in outs:
+        c.start()
+
+    heads = query_ref.shape[1]
+    q = query_ref[0].astype(jnp.float32)
+    q = q * rms(q) * query_gain_ref[...]
+    q = jnp.concatenate([q, q], axis=0).astype(jnp.bfloat16)
+    scores = lax.dot_general(
+        q, k_line[...], (((1,), (1,)), ((), ())), preferred_element_type=jnp.float32
+    )
+    scores = scores * (1.0 / head**0.5) + shifts
+    soft = jnp.log1p(jnp.exp(-jnp.abs(scores)))
+    log_keep = -(jnp.maximum(scores, 0.0) + soft)
+    log_stop = jnp.minimum(scores, 0.0) - soft
+    lanes = 128
+    count = scores.shape[1] // lanes
+    later = (
+        lax.broadcasted_iota(jnp.int32, (lanes, lanes), 0)
+        > lax.broadcasted_iota(jnp.int32, (lanes, lanes), 1)
+    ).astype(jnp.float32)
+    blocks = [log_keep[:, i * lanes : (i + 1) * lanes] for i in range(count)]
+    within = jnp.dot(
+        jnp.concatenate(blocks, axis=0),
+        later,
+        precision=lax.Precision.HIGHEST,
+        preferred_element_type=jnp.float32,
+    )
+    m = q.shape[0]
+    carry = jnp.zeros((m, 1), jnp.float32)
+    inside = [None] * count
+    for i in range(count - 1, -1, -1):
+        inside[i] = within[i * m : (i + 1) * m] + carry
+        carry = carry + jnp.sum(blocks[i], axis=1, keepdims=True)
+    weights = jnp.exp(log_stop + jnp.concatenate(inside, axis=1)).astype(jnp.bfloat16)
+    read = jnp.dot(weights, v_line[...], preferred_element_type=jnp.float32)[:heads]
+    read_out[0] = (read * rms(read) * out_gain_ref[...]).astype(jnp.bfloat16)
+
+    for c in outs:
+        c.wait()
+    for c in started:
+        c.wait_send()
+
+
+def lanes_of_cores(nx, nz, *args):
+    (x, gain, kw, vw, key_gain, shift, query, query_gain, out_gain) = args
+    tp = lax.axis_size("tp")
+    rows, width = x.shape[1:]
+    depth, head = kw.shape
+    sp = nx * nz
+    length = rows * tp
+    vmem = pl.BlockSpec(memory_space=pltpu.VMEM)
+    hbm = pl.BlockSpec(memory_space=pl.ANY)
+    bf16 = jnp.bfloat16
+    dma = lambda n: pltpu.SemaphoreType.DMA((2, n))
+    return pl.pallas_call(
+        functools.partial(fused, nx, nz),
+        out_shape=(
+            jax.ShapeDtypeStruct((1, 1, length, head), bf16),
+            jax.ShapeDtypeStruct((1, 1, length, head), bf16),
+            jax.ShapeDtypeStruct((1, 1, length), bf16),
+            jax.ShapeDtypeStruct(query.shape, bf16),
+        ),
+        in_specs=[hbm, vmem, hbm, hbm] + [vmem] * 5,
+        out_specs=(hbm, hbm, vmem, vmem),
+        scratch_shapes=[
+            pltpu.VMEM((CORES, rows, width), bf16),
+            pltpu.VMEM((CORES, rows, width), bf16),
+            pltpu.VMEM((tp // CORES, sp * depth, 2 * head), bf16),
+            pltpu.VMEM((CORES, rows, head), bf16),
+            pltpu.VMEM((CORES, rows, head), bf16),
+            pltpu.VMEM((length, head), bf16),
+            pltpu.VMEM((length, head), bf16),
+            pltpu.VMEM((tp,) + shift.shape[1:], bf16),
+            pltpu.SemaphoreType.DMA((3,)),
+            pltpu.SemaphoreType.DMA((2,)),
+            dma(1),
+            dma(3),
+            dma(nz - 1),
+            dma(nz),
+            dma(2 * nz),
+            dma(1),
+            dma(2),
+            dma(4 * (nz - 1)),
+            dma(2 * CORES),
+        ],
+        compiler_params=pltpu.CompilerParams(
+            collective_id=0, has_side_effects=True, vmem_limit_bytes=48 * 1024 * 1024
+        ),
+        name="fused",
+    )(
+        x,
+        gain.reshape(1, width),
+        kw,
+        vw,
+        key_gain.reshape(1, head),
+        shift,
+        query,
+        query_gain.reshape(1, head),
+        out_gain.reshape(1, head),
+    )
+
+
+def x_extent(mesh):
+    spots = [getattr(d, "coords", None) for d in mesh.devices.flat]
+    if any(s is None for s in spots):
+        return 2
+    return len({s[0] for s in spots})
+
 
 def solution(mesh):
+    nx = x_extent(mesh)
+    nz = mesh.shape["sp"] // nx
+    small = nx == 2 and mesh.shape["tp"] == KVH and nz > 1 and nx * nz == mesh.shape["sp"]
+    body = functools.partial(lanes_of_cores, nx, nz) if small else shards
     placed = (
         P("sp", "tp", None),
         P(),
@@ -91,7 +443,7 @@
         P(),
     )
     return jax.shard_map(
-        shards,
+        body,
         mesh=mesh,
         in_specs=placed,
         out_specs=(

time: 126 us -> 49 us (0.39)
  waiting for transfers between devices: 77.2 us -> 0 us
  Pallas kernels: 0 us -> 38.3 us
  between operations: 14.2 us -> 0.66 us
  other arithmetic: 11.1 us -> 0 us
  starting transfers between devices: 10.2 us -> 0 us
  matrix products: 5.2 us -> 0 us
  local copies, waits for them, and re-layouts: 7.15 us -> 9.75 us
    all_gather x2 -> x0, waiting for transfers between devices: 69.3 us -> none  [the longest x1 42.8 us: shards(): full_depth = lax.all_gather(stacked, 'sp', axis=1, tiled=True)]
    pallas_call x0 -> x1, Pallas kernels: none -> 38.3 us  [lanes_of_cores(): pl.pallas_call(functools.partial(fused, nx, nz), out_shape=(jax.ShapeDtyp...]
    all_to_all x3 -> x0, starting transfers between devices: 10.2 us -> none  [the longest x1 3.46 us: shards(): lax.all_to_all(key_slots, 'tp', split_axis=1, concat_axis=0, tiled=True)]
    all_to_all x3 -> x0, waiting for transfers between devices: 7.9 us -> none  [the longest x1 6.25 us: shards(): lax.all_to_all(key_slots, 'tp', split_axis=1, concat_axis=0, tiled=True)]
    another operation x3 -> x0, other arithmetic: 5.84 us -> none
    dot_general x3 -> x0, matrix products: 5.2 us -> none  [the longest x1 4.62 us: shards(): jnp.einsum('rd,kdc->krc', normed, lax.all_gather(full_depth, 'tp', axis=2...]
    unnamed x21 -> x22, local copies, waits for them, and re-layouts: 4.98 us -> 9.75 us
    reduce_sum x3 -> x0, other arithmetic: 2.82 us -> none  [row_norm(): jnp.mean(value_entries * value_entries, axis=-1, keepdims=True) + epsilon]
  transfers between devices with their start and end apart: 5 -> 0, of which waited for: 4 -> 0; matrix products, arithmetic and copies ran while one was open for 14% -> 0% of each run, Pallas kernels for 0% -> 0%
where the time goes in v1:
time: 49 us; the launch traced here: 48.7 us
  Pallas kernels  38.3 us (78%)
  local copies, waits for them, and re-layouts  9.75 us (20%)
  between operations  0.66 us (1%)
    pallas_call x1, Pallas kernels, lanes_of_cores(): pl.pallas_call(functools.partial(fused, nx, nz), out_shape=(jax.ShapeDtyp...  38.3 us
    unnamed x22, local copies, waits for them, and re-layouts  9.75 us

profile of v1, /device:TPU:0, one launch (start us, length us, event | category | flops | bytes accessed | tf_op | source)
XLA Modules:
  0.0 48.7 jit_solution(18033753636631574743)
XLA Ops:
  0.6 0.0 copy-start
  0.6 1.4 %copy-done = bf16[1,384,2048]{2,1,0:T(8,128)(2,1)S(1)} copy-done((bf16[1,384,2048]{2,1,0:T(8,128)(2,1)S(1)}, bf16[1,384,2048]{2,1,0:T(8,128)(2,1)}, u32[]{:S(2)}) %copy-start) | copy-done | bytes 1572888
  2.0 0.0 copy-start.1
  2.0 0.8 %copy-done.1 = bf16[256,128]{1,0:T(8,128)(2,1)S(1)} copy-done((bf16[256,128]{1,0:T(8,128)(2,1)S(1)}, bf16[256,128]{1,0:T(8,128)(2,1)}, u32[]{:S(2)}) %copy-start.1) | copy-done | bytes 65560
  2.9 0.0 copy-start.2
  2.9 0.8 %copy-done.2 = bf16[256,128]{1,0:T(8,128)(2,1)S(1)} copy-done((bf16[256,128]{1,0:T(8,128)(2,1)S(1)}, bf16[256,128]{1,0:T(8,128)(2,1)}, u32[]{:S(2)}) %copy-start.2) | copy-done | bytes 65560
  3.7 0.0 copy-start.3
  3.7 0.7 %copy-done.3 = f32[2048]{0:T(1024)S(1)} copy-done((f32[2048]{0:T(1024)S(1)}, f32[2048]{0:T(1024)}, u32[]{:S(2)}) %copy-start.3) | copy-done | bytes 8216
  4.4 0.0 copy-start.4
  4.4 0.7 %copy-done.4 = bf16[1,4,384]{2,1,0:T(4,128)(2,1)S(1)} copy-done((bf16[1,4,384]{2,1,0:T(4,128)(2,1)S(1)}, bf16[1,4,384]{2,1,0:T(4,128)(2,1)}, u32[]{:S(2)}) %copy-start.4) | copy-done | bytes 3096
  5.1 0.0 copy-start.5
  5.1 0.7 %copy-done.5 = bf16[1,4,128]{2,1,0:T(4,128)(2,1)S(1)} copy-done((bf16[1,4,128]{2,1,0:T(4,128)(2,1)S(1)}, bf16[1,4,128]{2,1,0:T(4,128)(2,1)}, u32[]{:S(2)}) %copy-start.5) | copy-done | bytes 1048
  5.8 0.0 copy-start.6
  5.8 0.7 %copy-done.6 = f32[128]{0:T(128)S(1)} copy-done((f32[128]{0:T(128)S(1)}, f32[128]{0:T(128)}, u32[]{:S(2)}) %copy-start.6) | copy-done | bytes 536
  6.4 0.0 copy-start.7
  6.4 0.7 %copy-done.7 = f32[128]{0:T(128)S(1)} copy-done((f32[128]{0:T(128)S(1)}, f32[128]{0:T(128)}, u32[]{:S(2)}) %copy-start.7) | copy-done | bytes 536
  7.1 0.0 copy-start.8
  7.1 0.7 %copy-done.8 = f32[128]{0:T(128)S(1)} copy-done((f32[128]{0:T(128)S(1)}, f32[128]{0:T(128)}, u32[]{:S(2)}) %copy-start.8) | copy-done | bytes 536
  7.8 38.3 %fused.1 = (bf16[1,1,1536,128]{3,2,1,0:T(8,128)(2,1)S(1)}, bf16[1,1,1536,128]{3,2,1,0:T(8,128)(2,1)S(1)}, bf16[1,1,1536]{2,1,0:T(2,128)(2,1)S(1)}, bf16[1,4,128]{2,1,0:T(4,128)(2,1)S(1)}) custom-call(bf16[1,384,2048]{2,1,0:T(8,128)(2,1)S(1)} %copy-done, f32[1,2048]{1,0:T(1,128)S(1)} %bitcast.4, bf16[256,128]{1,0:T(8,128)(2,1)S(1)} %copy-done.1, ...), custom_call_target="tpu_custom_call" | custom-call | tf_op jit(solution)/shard_map/fused/pallas_call | solution.py:374
  46.0 0.7 %copy.17 = bf16[1,1,1536,128]{3,2,1,0:T(8,128)(2,1)} copy(bf16[1,1,1536,128]{3,2,1,0:T(8,128)(2,1)S(1)} %get-tuple-element.8) | data formatting | bytes 786432
  46.8 0.7 %copy.18 = bf16[1,1,1536,128]{3,2,1,0:T(8,128)(2,1)} copy(bf16[1,1,1536,128]{3,2,1,0:T(8,128)(2,1)S(1)} %get-tuple-element.9) | data formatting | bytes 786432
  47.5 0.6 %copy.19 = bf16[1,1,1536]{2,1,0:T(2,128)(2,1)} copy(bf16[1,1,1536]{2,1,0:T(2,128)(2,1)S(1)} %get-tuple-element.10) | data formatting | bytes 6144
  48.1 0.6 %copy.20 = bf16[1,4,128]{2,1,0:T(4,128)(2,1)} copy(bf16[1,4,128]{2,1,0:T(4,128)(2,1)S(1)} %get-tuple-element.11) | data formatting | bytes 2048
Async XLA Ops:
  0.6 1.4 %copy-start = (bf16[1,384,2048]{2,1,0:T(8,128)(2,1)S(1)}, bf16[1,384,2048]{2,1,0:T(8,128)(2,1)}, u32[]{:S(2)}) copy-start(bf16[1,384,2048]{2,1,0:T(8,128)(2,1)} %x_ref.1) | copy-start | bytes 4718596
  2.0 0.8 %copy-start.1 = (bf16[256,128]{1,0:T(8,128)(2,1)S(1)}, bf16[256,128]{1,0:T(8,128)(2,1)}, u32[]{:S(2)}) copy-start(bf16[256,128]{1,0:T(8,128)(2,1)} %kw_ref.1) | copy-start | bytes 196612
  2.9 0.8 %copy-start.2 = (bf16[256,128]{1,0:T(8,128)(2,1)S(1)}, bf16[256,128]{1,0:T(8,128)(2,1)}, u32[]{:S(2)}) copy-start(bf16[256,128]{1,0:T(8,128)(2,1)} %vw_ref.1) | copy-start | bytes 196612
  3.7 0.7 %copy-start.3 = (f32[2048]{0:T(1024)S(1)}, f32[2048]{0:T(1024)}, u32[]{:S(2)}) copy-start(f32[2048]{0:T(1024)} %param.10) | copy-start | bytes 24580
  4.4 0.7 %copy-start.4 = (bf16[1,4,384]{2,1,0:T(4,128)(2,1)S(1)}, bf16[1,4,384]{2,1,0:T(4,128)(2,1)}, u32[]{:S(2)}) copy-start(bf16[1,4,384]{2,1,0:T(4,128)(2,1)} %shift_ref.1) | copy-start | bytes 9220
  5.1 0.7 %copy-start.5 = (bf16[1,4,128]{2,1,0:T(4,128)(2,1)S(1)}, bf16[1,4,128]{2,1,0:T(4,128)(2,1)}, u32[]{:S(2)}) copy-start(bf16[1,4,128]{2,1,0:T(4,128)(2,1)} %query_ref.1) | copy-start | bytes 3076
  5.8 0.7 %copy-start.6 = (f32[128]{0:T(128)S(1)}, f32[128]{0:T(128)}, u32[]{:S(2)}) copy-start(f32[128]{0:T(128)} %param.13) | copy-start | bytes 1540
  6.4 0.7 %copy-start.7 = (f32[128]{0:T(128)S(1)}, f32[128]{0:T(128)}, u32[]{:S(2)}) copy-start(f32[128]{0:T(128)} %param.16) | copy-start | bytes 1540
  7.1 0.7 %copy-start.8 = (f32[128]{0:T(128)S(1)}, f32[128]{0:T(128)}, u32[]{:S(2)}) copy-start(f32[128]{0:T(128)} %param.17) | copy-start | bytes 1540

commit v2 on v0

--- a/solution.py
+++ b/solution.py
@@ -1,6 +1,10 @@
+import functools
+
 import jax
 import jax.numpy as jnp
 from jax import lax
+from jax.experimental import pallas as pl
+from jax.experimental.pallas import tpu as pltpu
 from jax.sharding import PartitionSpec as P
 
 KVH = 4
@@ -77,8 +81,385 @@
         first_out[None],
     )
 
+CORES = 2
+VMEM_LIMIT = 67043328
+
+
+def rms(entries):
+    return lax.rsqrt(jnp.mean(entries * entries, axis=-1, keepdims=True) + epsilon)
+
+
+def gather_kernel(
+    nx,
+    nz,
+    x_ref,
+    gain_ref,
+    kw_ref,
+    vw_ref,
+    key_gain_ref,
+    shift_ref,
+    k_line,
+    v_line,
+    shift_buf,
+    x_buf,
+    n_buf,
+    k_buf,
+    v_buf,
+    k_send,
+    v_send,
+    gain_buf,
+    key_gain_buf,
+    local_sem,
+    act_sem,
+    shift_sem,
+    zk_sem,
+    yk_sem,
+    xk_sem,
+    yv_sem,
+    zv_sem,
+    xv_sem,
+    kv_sem,
+):
+    sp, tp = lax.axis_index("sp"), lax.axis_index("tp")
+    z, x = sp // nx, sp % nx
+    y, core = tp // CORES, tp % CORES
+    rows = x_ref.shape[1]
+    depth = kw_ref.shape[0]
+    far_y = 1 - y
+
+    def device(zz, xx, yy, cc):
+        return (zz * nx + xx, yy * CORES + cc)
+
+    def zs(d):
+        return lax.rem(z + d, nz)
+
+    def zb(d):
+        return lax.rem(z + nz - d, nz) if d else z
+
+    partner = device(z, x, y, 1 - core)
+    y_peer = device(z, x, far_y, core)
+    x_peer = device(z, 1 - x, y, core)
+    z_peers = [device(zs(d), x, y, core) for d in range(1, nz)]
+    cross = device(z, x, far_y, 1 - core)
+
+    own = pl.multiple_of(sp * depth, depth)
+    locals_ = [
+        pltpu.make_async_copy(kw_ref, k_buf.at[y, pl.ds(own, depth), :], local_sem.at[0]),
+        pltpu.make_async_copy(vw_ref, v_buf.at[y, pl.ds(own, depth), :], local_sem.at[1]),
+        pltpu.make_async_copy(x_ref.at[0], x_buf.at[core], local_sem.at[2]),
+        pltpu.make_async_copy(gain_ref, gain_buf, local_sem.at[3]),
+        pltpu.make_async_copy(key_gain_ref, key_gain_buf, local_sem.at[4]),
+        pltpu.make_async_copy(shift_ref.at[0], shift_buf.at[tp], local_sem.at[5]),
+    ]
+    for c in locals_:
+        c.start()
+
+    barrier = pltpu.get_barrier_semaphore()
+    greeted = [partner, y_peer, x_peer, cross] + z_peers
+    for peer in greeted:
+        pl.semaphore_signal(
+            barrier, inc=1, device_id=peer, device_id_type=pl.DeviceIdType.MESH
+        )
+    pl.semaphore_wait(barrier, len(greeted))
+
+    started = []
+
+    def remote(src, dst, sems, index, peer):
+        return pltpu.make_async_remote_copy(
+            src_ref=src,
+            dst_ref=dst,
+            send_sem=sems.at[0, index],
+            recv_sem=sems.at[1, index],
+            device_id=peer,
+            device_id_type=pl.DeviceIdType.MESH,
+        )
+
+    def send(src, dst, sems, index, peer):
+        c = remote(src, dst, sems, index, peer)
+        c.start()
+        started.append(c)
+
+    def arrived(dst, sems, index, peer):
+        remote(dst, dst, sems, index, peer).wait_recv()
+
+    def part(buf, zz, xx, yy):
+        at = pl.multiple_of((zz * nx + xx) * depth, depth)
+        return buf.at[yy, pl.ds(at, depth), :]
+
+    def pass_on(block, sems, index, peer):
+        send(block, block, sems, index, peer)
+
+    locals_[0].wait()
+    k_own = part(k_buf, z, x, y)
+    pass_on(k_own, yk_sem, 0, y_peer)
+    pass_on(k_own, xk_sem, 0, x_peer)
+    for d in range(1, nz):
+        pass_on(k_own, zk_sem, d - 1, z_peers[d - 1])
+    locals_[1].wait()
+    v_own = part(v_buf, z, x, y)
+    pass_on(v_own, yv_sem, 0, y_peer)
+    pass_on(v_own, xv_sem, 0, x_peer)
+    send(x_ref.at[0], x_buf.at[core], act_sem, 0, partner)
+    for i, peer in enumerate((partner, y_peer, cross)):
+        send(shift_ref.at[0], shift_buf.at[tp], shift_sem, i, peer)
+
+    tile = 16
+
+    def normalise(which, first, last):
+        def body(i, _):
+            at = pl.multiple_of(i * tile, tile)
+            v = x_buf[which, pl.ds(at, tile), :].astype(jnp.float32)
+            n_buf[which, pl.ds(at, tile), :] = (v * rms(v) * gain_buf[...]).astype(jnp.bfloat16)
+            return 0
+
+        lax.fori_loop(first, last, body, 0, unroll=2)
+
+    for c in locals_[2:]:
+        c.wait()
+    tiles = rows // tile
+    normalise(core, 0, tiles)
+
+    arrived(part(k_buf, z, x, far_y), yk_sem, 0, y_peer)
+    pass_on(part(k_buf, z, x, far_y), xk_sem, nz, x_peer)
+    arrived(part(v_buf, z, x, far_y), yv_sem, 0, y_peer)
+    for d in range(1, nz):
+        pass_on(part(v_buf, z, x, far_y), zv_sem, nz - 1 + d - 1, z_peers[d - 1])
+    for d in range(1, nz):
+        pass_on(v_own, zv_sem, d - 1, z_peers[d - 1])
+    for d in range(1, nz):
+        block = part(k_buf, zb(d), x, y)
+        arrived(block, zk_sem, d - 1, z_peers[nz - d - 1])
+        pass_on(block, yk_sem, d, y_peer)
+        if d == 1:
+            pass_on(part(v_buf, z, x, far_y), xv_sem, nz, x_peer)
+            pass_on(block, xk_sem, d, x_peer)
+            arrived(x_buf.at[1 - core], act_sem, 0, partner)
+        first = (d - 1) * tiles // (nz - 1) // 2 * 2
+        last = tiles if d == nz - 1 else d * tiles // (nz - 1) // 2 * 2
+        normalise(1 - core, first, last)
+    for d in range(1, nz):
+        block = part(k_buf, zb(d), x, far_y)
+        arrived(block, yk_sem, d, y_peer)
+        pass_on(block, xk_sem, nz + d, x_peer)
+    for d in range(1, nz):
+        block = part(v_buf, zb(d), x, far_y)
+        arrived(block, zv_sem, nz - 1 + d - 1, z_peers[nz - d - 1])
+        pass_on(block, xv_sem, nz + d, x_peer)
+    for d in range(2, nz):
+        pass_on(part(k_buf, zb(d), x, y), xk_sem, d, x_peer)
+
+    def keys_of(which, yy):
+        keys = jnp.dot(n_buf[which], k_buf[yy], preferred_element_type=jnp.float32)
+        return (keys * rms(keys) * key_gain_buf[...]).astype(jnp.bfloat16)
+
+    def values_of(which, yy):
+        return jnp.dot(n_buf[which], v_buf[yy], preferred_element_type=jnp.float32).astype(
+            jnp.bfloat16
+        )
+
+    def span(yy, c):
+        return pl.ds(pl.multiple_of((yy * CORES + c) * rows, rows), rows)
+
+    for d in range(nz):
+        arrived(part(k_buf, zb(d), 1 - x, far_y), xk_sem, nz + d, x_peer)
+    for c in range(CORES):
+        k_send[c] = keys_of(c, far_y)
+        send(k_send.at[c], k_line.at[span(y, c), :], kv_sem, c, y_peer)
+    for d in range(nz):
+        arrived(part(v_buf, zb(d), 1 - x, far_y), xv_sem, nz + d, x_peer)
+    for c in range(CORES):
+        v_send[c] = values_of(c, far_y)
+        send(v_send.at[c], v_line.at[span(y, c), :], kv_sem, CORES + c, y_peer)
+    for d in range(1, nz):
+        block = part(v_buf, zb(d), x, y)
+        arrived(block, zv_sem, d - 1, z_peers[nz - d - 1])
+        pass_on(block, xv_sem, d, x_peer)
+
+    for d in range(nz):
+        arrived(part(k_buf, zb(d), 1 - x, y), xk_sem, d, x_peer)
+    for c in range(CORES):
+        k_line[span(y, c), :] = keys_of(c, y)
+    for d in range(nz):
+        arrived(part(v_buf, zb(d), 1 - x, y), xv_sem, d, x_peer)
+    for c in range(CORES):
+        v_line[span(y, c), :] = values_of(c, y)
+
+    arrived(shift_buf.at[y * CORES + 1 - core], shift_sem, 0, partner)
+    arrived(shift_buf.at[far_y * CORES + core], shift_sem, 1, y_peer)
+    arrived(shift_buf.at[far_y * CORES + 1 - core], shift_sem, 2, cross)
+    for c in range(CORES):
+        arrived(k_line.at[span(far_y, c), :], kv_sem, c, y_peer)
+        arrived(v_line.at[span(far_y, c), :], kv_sem, CORES + c, y_peer)
+    for c in started:
+        c.wait_send()
+
+
+def read_kernel(
+    k_line,
+    v_line,
+    shift_buf,
+    query_ref,
+    query_gain_ref,
+    out_gain_ref,
+    key_out,
+    value_out,
+    shift_out,
+    read_out,
+    query_buf,
+    query_gain_buf,
+    out_gain_buf,
+    shift_line,
+    read_line,
+    in_sem,
+    out_sem,
+):
+    ins = [
+        pltpu.make_async_copy(query_ref, query_buf, in_sem.at[0]),
+        pltpu.make_async_copy(query_gain_ref, query_gain_buf, in_sem.at[1]),
+        pltpu.make_async_copy(out_gain_ref, out_gain_buf, in_sem.at[2]),
+    ]
+    outs = [
+        pltpu.make_async_copy(k_line, key_out.at[0, 0], out_sem.at[0]),
+        pltpu.make_async_copy(v_line, value_out.at[0, 0], out_sem.at[1]),
+        pltpu.make_async_copy(shift_line, shift_out, out_sem.at[2]),
+        pltpu.make_async_copy(read_line, read_out, out_sem.at[3]),
+    ]
+    for c in ins:
+        c.start()
+    outs[0].start()
+    outs[1].start()
+    tp = lax.axis_index("tp")
+    head = k_line.shape[1]
+    pieces = []
+    for t in range(shift_buf.shape[0]):
+        block = shift_buf[t].astype(jnp.float32)
+        mine = lax.broadcasted_iota(jnp.int32, block.shape, 0) == tp
+        pieces.append(jnp.sum(jnp.where(mine, block, 0.0), axis=0, keepdims=True))
+    shifts = jnp.concatenate(pieces, axis=1)
+    shift_line[0] = shifts.astype(jnp.bfloat16)
+    outs[2].start()
+    for c in ins:
+        c.wait()
+
+    heads = query_buf.shape[1]
+    q = query_buf[0].astype(jnp.float32)
+    q = q * rms(q) * query_gain_buf[...]
+    q = jnp.concatenate([q, q], axis=0).astype(jnp.bfloat16)
+    scores = lax.dot_general(
+        q, k_line[...], (((1,), (1,)), ((), ())), preferred_element_type=jnp.float32
+    )
+    scores = scores * (1.0 / head**0.5) + shifts
+    soft = jnp.log1p(jnp.exp(-jnp.abs(scores)))
+    log_keep = -(jnp.maximum(scores, 0.0) + soft)
+    log_stop = jnp.minimum(scores, 0.0) - soft
+    lanes = 128
+    count = scores.shape[1] // lanes
+    later = (
+        lax.broadcasted_iota(jnp.int32, (lanes, lanes), 0)
+        > lax.broadcasted_iota(jnp.int32, (lanes, lanes), 1)
+    ).astype(jnp.float32)
+    blocks = [log_keep[:, i * lanes : (i + 1) * lanes] for i in range(count)]
+    within = jnp.dot(
+        jnp.concatenate(blocks, axis=0),
+        later,
+        precision=lax.Precision.HIGHEST,
+        preferred_element_type=jnp.float32,
+    )
+    m = q.shape[0]
+    carry = jnp.zeros((m, 1), jnp.float32)
+    inside = [None] * count
+    for i in range(count - 1, -1, -1):
+        inside[i] = within[i * m : (i + 1) * m] + carry
+        carry = carry + jnp.sum(blocks[i], axis=1, keepdims=True)
+    weights = jnp.exp(log_stop + jnp.concatenate(inside, axis=1)).astype(jnp.bfloat16)
+    read = jnp.dot(weights, v_line[...], preferred_element_type=jnp.float32)[:heads]
+    read_line[0] = (read * rms(read) * out_gain_buf[...]).astype(jnp.bfloat16)
+    outs[3].start()
+    for c in outs:
+        c.wait()
+
+
+def lanes_of_cores(nx, nz, *args):
+    (x, gain, kw, vw, key_gain, shift, query, query_gain, out_gain) = args
+    tp = lax.axis_size("tp")
+    rows, width = x.shape[1:]
+    depth, head = kw.shape
+    sp = nx * nz
+    length = rows * tp
+    vmem = pl.BlockSpec(memory_space=pltpu.VMEM)
+    hbm = pl.BlockSpec(memory_space=pltpu.HBM)
+    bf16 = jnp.bfloat16
+    dma = lambda n: pltpu.SemaphoreType.DMA((2, n))
+    k_line, v_line, shifts = pl.pallas_call(
+        functools.partial(gather_kernel, nx, nz),
+        out_shape=(
+            jax.ShapeDtypeStruct((length, head), bf16),
+            jax.ShapeDtypeStruct((length, head), bf16),
+            jax.ShapeDtypeStruct((tp,) + shift.shape[1:], bf16),
+        ),
+        in_specs=[hbm] * 6,
+        out_specs=(vmem, vmem, vmem),
+        scratch_shapes=[
+            pltpu.VMEM((CORES, rows, width), bf16),
+            pltpu.VMEM((CORES, rows, width), bf16),
+            pltpu.VMEM((tp // CORES, sp * depth, head), bf16),
+            pltpu.VMEM((tp // CORES, sp * depth, head), bf16),
+            pltpu.VMEM((CORES, rows, head), bf16),
+            pltpu.VMEM((CORES, rows, head), bf16),
+            pltpu.VMEM((1, width), jnp.float32),
+            pltpu.VMEM((1, head), jnp.float32),
+            pltpu.SemaphoreType.DMA((6,)),
+            dma(1),
+            dma(3),
+            dma(nz - 1),
+            dma(nz),
+            dma(2 * nz),
+            dma(1),
+            dma(2 * (nz - 1)),
+            dma(2 * nz),
+            dma(2 * CORES),
+        ],
+        compiler_params=pltpu.CompilerParams(
+            collective_id=0, has_side_effects=True, vmem_limit_bytes=VMEM_LIMIT
+        ),
+        name="gather_project",
+    )(x, gain.reshape(1, width), kw, vw, key_gain.reshape(1, head), shift)
+    return pl.pallas_call(
+        read_kernel,
+        out_shape=(
+            jax.ShapeDtypeStruct((1, 1, length, head), bf16),
+            jax.ShapeDtypeStruct((1, 1, length, head), bf16),
+            jax.ShapeDtypeStruct((1, 1, length), bf16),
+            jax.ShapeDtypeStruct(query.shape, bf16),
+        ),
+        in_specs=[vmem] * 3 + [hbm] * 3,
+        out_specs=(hbm,) * 4,
+        scratch_shapes=[
+            pltpu.VMEM(query.shape, bf16),
+            pltpu.VMEM((1, head), jnp.float32),
+            pltpu.VMEM((1, head), jnp.float32),
+            pltpu.VMEM((1, 1, length), bf16),
+            pltpu.VMEM(query.shape, bf16),
+            pltpu.SemaphoreType.DMA((3,)),
+            pltpu.SemaphoreType.DMA((4,)),
+        ],
+        compiler_params=pltpu.CompilerParams(vmem_limit_bytes=VMEM_LIMIT),
+        name="read",
+    )(k_line, v_line, shifts, query, query_gain.reshape(1, head), out_gain.reshape(1, head))
+
+
+def x_extent(mesh):
+    spots = [getattr(d, "coords", None) for d in mesh.devices.flat]
+    if any(s is None for s in spots):
+        return 2
+    return len({s[0] for s in spots})
+
 
 def solution(mesh):
+    nx = x_extent(mesh)
+    nz = mesh.shape["sp"] // nx
+    small = nx == 2 and mesh.shape["tp"] == KVH and nz > 1 and nx * nz == mesh.shape["sp"]
+    body = functools.partial(lanes_of_cores, nx, nz) if small else shards
     placed = (
         P("sp", "tp", None),
         P(),
@@ -91,7 +472,7 @@
         P(),
     )
     return jax.shard_map(
-        shards,
+        body,
         mesh=mesh,
         in_specs=placed,
         out_specs=(

time: 126 us -> 38.6 us (0.31)
  the two profiles are of different devices: /device:TPU:0 before, /device:TPU:10 now
where the time goes in v2:
time: 38.6 us; the launch traced here: 38.5 us
  Pallas kernels  37.8 us (98%)
  between operations  0.64 us (2%)
    pallas_call x1, Pallas kernels, lanes_of_cores(): pl.pallas_call(functools.partial(gather_kernel, nx, nz), out_shape=(jax.S...  34.6 us
    pallas_call x1, Pallas kernels, lanes_of_cores(): pl.pallas_call(read_kernel, out_shape=(jax.ShapeDtypeStruct((1, 1, length...  3.28 us

profile of v2, /device:TPU:10, one launch (start us, length us, event | category | flops | bytes accessed | tf_op | source)
XLA Modules:
  0.0 38.5 jit_solution(8894607958320376453)
XLA Ops:
  0.6 34.6 %gather_project.1 = (bf16[1536,128]{1,0:T(8,128)(2,1)}, bf16[1536,128]{1,0:T(8,128)(2,1)}, bf16[4,4,384]{2,1,0:T(4,128)(2,1)}) custom-call(bf16[1,384,2048]{2,1,0:T(8,128)(2,1)} %x_ref.1, f32[1,2048]{1,0:T(1,128)} %bitcast.4, bf16[256,128]{1,0:T(8,128)(2,1)} %kw_ref.1, bf16[256,128]{1,0:T(8,128)(2,1)} %vw_ref.1, f32[1,128]{1,0:T(1,128)} %bitcast.5, ...), custom_call_target="tpu_custom_call" | custom-call | tf_op jit(solution)/shard_map/gather_project/pallas_call | solution.py:393
  35.2 3.3 %read.1 = (bf16[1,1,1536,128]{3,2,1,0:T(8,128)(2,1)}, bf16[1,1,1536,128]{3,2,1,0:T(8,128)(2,1)}, bf16[1,1,1536]{2,1,0:T(2,128)(2,1)}, bf16[1,4,128]{2,1,0:T(4,128)(2,1)}) custom-call(bf16[1536,128]{1,0:T(8,128)(2,1)} %get-tuple-element.7.k_line, bf16[1536,128]{1,0:T(8,128)(2,1)} %get-tuple-element.8.v_line, bf16[4,4,384]{2,1,0:T(4,128)(2,1)} %get-tuple-element.9.shift_buf, ...), custom_call_target="tpu_custom_call" | custom-call | tf_op jit(solution)/shard_map/read/pallas_call | solution.py:427

commit v3 on v2

--- a/solution.py
+++ b/solution.py
@@ -82,6 +82,7 @@
     )
 
 CORES = 2
+Z_EIGHTHS = 2
 VMEM_LIMIT = 67043328
 
 
@@ -98,9 +99,15 @@
     vw_ref,
     key_gain_ref,
     shift_ref,
+    query_ref,
+    query_gain_ref,
     k_line,
     v_line,
+    shift_line,
+    weight_line,
     shift_buf,
+    query_buf,
+    query_gain_buf,
     x_buf,
     n_buf,
     k_buf,
@@ -150,6 +157,8 @@
         pltpu.make_async_copy(gain_ref, gain_buf, local_sem.at[3]),
         pltpu.make_async_copy(key_gain_ref, key_gain_buf, local_sem.at[4]),
         pltpu.make_async_copy(shift_ref.at[0], shift_buf.at[tp], local_sem.at[5]),
+        pltpu.make_async_copy(query_ref, query_buf, local_sem.at[6]),
+        pltpu.make_async_copy(query_gain_ref, query_gain_buf, local_sem.at[7]),
     ]
     for c in locals_:
         c.start()
@@ -186,6 +195,12 @@
         at = pl.multiple_of((zz * nx + xx) * depth, depth)
         return buf.at[yy, pl.ds(at, depth), :]
 
+    def half(zz, xx, yy, i):
+        cut = depth * Z_EIGHTHS // 8
+        first, size = ((0, depth - cut), (depth - cut, cut))[i]
+        at = pl.multiple_of((zz * nx + xx) * depth + first, depth // 8)
+        return v_buf.at[yy, pl.ds(at, size), :]
+
     def pass_on(block, sems, index, peer):
         send(block, block, sems, index, peer)
 
@@ -219,8 +234,8 @@
     tiles = rows // tile
     normalise(core, 0, tiles)
 
-    arrived(part(k_buf, z, x, far_y), yk_sem, 0, y_peer)
-    pass_on(part(k_buf, z, x, far_y), xk_sem, nz, x_peer)
+    arrived(part(k_buf, z, 1 - x, y), xk_sem, 0, x_peer)
+    pass_on(part(k_buf, z, 1 - x, y), yk_sem, nz, y_peer)
     arrived(part(v_buf, z, x, far_y), yv_sem, 0, y_peer)
     for d in range(1, nz):
         pass_on(part(v_buf, z, x, far_y), zv_sem, nz - 1 + d - 1, z_peers[d - 1])
@@ -230,23 +245,24 @@
         block = part(k_buf, zb(d), x, y)
         arrived(block, zk_sem, d - 1, z_peers[nz - d - 1])
         pass_on(block, yk_sem, d, y_peer)
+        pass_on(block, xk_sem, d, x_peer)
         if d == 1:
             pass_on(part(v_buf, z, x, far_y), xv_sem, nz, x_peer)
-            pass_on(block, xk_sem, d, x_peer)
+            arrived(part(v_buf, z, 1 - x, y), xv_sem, 0, x_peer)
+            for e in range(1, nz):
+                pass_on(half(z, 1 - x, y, 1), zv_sem, 2 * (nz - 1) + e - 1, z_peers[e - 1])
             arrived(x_buf.at[1 - core], act_sem, 0, partner)
         first = (d - 1) * tiles // (nz - 1) // 2 * 2
         last = tiles if d == nz - 1 else d * tiles // (nz - 1) // 2 * 2
         normalise(1 - core, first, last)
     for d in range(1, nz):
-        block = part(k_buf, zb(d), x, far_y)
-        arrived(block, yk_sem, d, y_peer)
-        pass_on(block, xk_sem, nz + d, x_peer)
+        block = part(k_buf, zb(d), 1 - x, y)
+        arrived(block, xk_sem, d, x_peer)
+        pass_on(block, yk_sem, nz + d, y_peer)
     for d in range(1, nz):
         block = part(v_buf, zb(d), x, far_y)
         arrived(block, zv_sem, nz - 1 + d - 1, z_peers[nz - d - 1])
         pass_on(block, xv_sem, nz + d, x_peer)
-    for d in range(2, nz):
-        pass_on(part(k_buf, zb(d), x, y), xk_sem, d, x_peer)
 
     def keys_of(which, yy):
         keys = jnp.dot(n_buf[which], k_buf[yy], preferred_element_type=jnp.float32)
@@ -261,75 +277,28 @@
         return pl.ds(pl.multiple_of((yy * CORES + c) * rows, rows), rows)
 
     for d in range(nz):
-        arrived(part(k_buf, zb(d), 1 - x, far_y), xk_sem, nz + d, x_peer)
+        arrived(part(k_buf, zb(d), x, far_y), yk_sem, d, y_peer)
+        arrived(part(k_buf, zb(d), 1 - x, far_y), yk_sem, nz + d, y_peer)
     for c in range(CORES):
         k_send[c] = keys_of(c, far_y)
         send(k_send.at[c], k_line.at[span(y, c), :], kv_sem, c, y_peer)
+    for d in range(1, nz):
+        block = part(v_buf, zb(d), x, y)
+        arrived(block, zv_sem, d - 1, z_peers[nz - d - 1])
+        pass_on(half(zb(d), x, y, 0), xv_sem, d, x_peer)
     for d in range(nz):
         arrived(part(v_buf, zb(d), 1 - x, far_y), xv_sem, nz + d, x_peer)
     for c in range(CORES):
         v_send[c] = values_of(c, far_y)
         send(v_send.at[c], v_line.at[span(y, c), :], kv_sem, CORES + c, y_peer)
-    for d in range(1, nz):
-        block = part(v_buf, zb(d), x, y)
-        arrived(block, zv_sem, d - 1, z_peers[nz - d - 1])
-        pass_on(block, xv_sem, d, x_peer)
-
-    for d in range(nz):
-        arrived(part(k_buf, zb(d), 1 - x, y), xk_sem, d, x_peer)
+
     for c in range(CORES):
         k_line[span(y, c), :] = keys_of(c, y)
-    for d in range(nz):
-        arrived(part(v_buf, zb(d), 1 - x, y), xv_sem, d, x_peer)
-    for c in range(CORES):
-        v_line[span(y, c), :] = values_of(c, y)
-
     arrived(shift_buf.at[y * CORES + 1 - core], shift_sem, 0, partner)
     arrived(shift_buf.at[far_y * CORES + core], shift_sem, 1, y_peer)
     arrived(shift_buf.at[far_y * CORES + 1 - core], shift_sem, 2, cross)
     for c in range(CORES):
         arrived(k_line.at[span(far_y, c), :], kv_sem, c, y_peer)
-        arrived(v_line.at[span(far_y, c), :], kv_sem, CORES + c, y_peer)
-    for c in started:
-        c.wait_send()
-
-
-def read_kernel(
-    k_line,
-    v_line,
-    shift_buf,
-    query_ref,
-    query_gain_ref,
-    out_gain_ref,
-    key_out,
-    value_out,
-    shift_out,
-    read_out,
-    query_buf,
-    query_gain_buf,
-    out_gain_buf,
-    shift_line,
-    read_line,
-    in_sem,
-    out_sem,
-):
-    ins = [
-        pltpu.make_async_copy(query_ref, query_buf, in_sem.at[0]),
-        pltpu.make_async_copy(query_gain_ref, query_gain_buf, in_sem.at[1]),
-        pltpu.make_async_copy(out_gain_ref, out_gain_buf, in_sem.at[2]),
-    ]
-    outs = [
-        pltpu.make_async_copy(k_line, key_out.at[0, 0], out_sem.at[0]),
-        pltpu.make_async_copy(v_line, value_out.at[0, 0], out_sem.at[1]),
-        pltpu.make_async_copy(shift_line, shift_out, out_sem.at[2]),
-        pltpu.make_async_copy(read_line, read_out, out_sem.at[3]),
-    ]
-    for c in ins:
-        c.start()
-    outs[0].start()
-    outs[1].start()
-    tp = lax.axis_index("tp")
-    head = k_line.shape[1]
     pieces = []
     for t in range(shift_buf.shape[0]):
         block = shift_buf[t].astype(jnp.float32)
@@ -337,11 +306,7 @@
         pieces.append(jnp.sum(jnp.where(mine, block, 0.0), axis=0, keepdims=True))
     shifts = jnp.concatenate(pieces, axis=1)
     shift_line[0] = shifts.astype(jnp.bfloat16)
-    outs[2].start()
-    for c in ins:
-        c.wait()
-
-    heads = query_buf.shape[1]
+    head = k_line.shape[1]
     q = query_buf[0].astype(jnp.float32)
     q = q * rms(q) * query_gain_buf[...]
     q = jnp.concatenate([q, q], axis=0).astype(jnp.bfloat16)
@@ -371,9 +336,62 @@
     for i in range(count - 1, -1, -1):
         inside[i] = within[i * m : (i + 1) * m] + carry
         carry = carry + jnp.sum(blocks[i], axis=1, keepdims=True)
-    weights = jnp.exp(log_stop + jnp.concatenate(inside, axis=1)).astype(jnp.bfloat16)
-    read = jnp.dot(weights, v_line[...], preferred_element_type=jnp.float32)[:heads]
-    read_line[0] = (read * rms(read) * out_gain_buf[...]).astype(jnp.bfloat16)
+    weight_line[...] = jnp.exp(log_stop + jnp.concatenate(inside, axis=1)).astype(jnp.bfloat16)
+
+    for d in range(1, nz):
+        arrived(half(zb(d), 1 - x, y, 0), xv_sem, d, x_peer)
+        arrived(
+            half(zb(d), 1 - x, y, 1), zv_sem, 2 * (nz - 1) + d - 1, z_peers[nz - d - 1]
+        )
+    for c in range(CORES):
+        v_line[span(y, c), :] = values_of(c, y)
+    for c in range(CORES):
+        arrived(v_line.at[span(far_y, c), :], kv_sem, CORES + c, y_peer)
+    for c in started:
+        c.wait_send()
+
+
+def read_kernel(
+    k_line,
+    v_line,
+    shift_line,
+    weight_line,
+    out_gain_ref,
+    key_out,
+    value_out,
+    shift_out,
+    read_out,
+    k_buf,
+    v_buf,
+    s_buf,
+    w_buf,
+    gain_buf,
+    read_line,
+    in_sem,
+    out_sem,
+):
+    pairs = [(v_line, v_buf), (weight_line, w_buf), (out_gain_ref, gain_buf)]
+    pairs += [(k_line, k_buf), (shift_line, s_buf)]
+    ins = [pltpu.make_async_copy(a, b, in_sem.at[i]) for i, (a, b) in enumerate(pairs)]
+    outs = [
+        pltpu.make_async_copy(v_buf, value_out.at[0, 0], out_sem.at[1]),
+        pltpu.make_async_copy(k_buf, key_out.at[0, 0], out_sem.at[0]),
+        pltpu.make_async_copy(s_buf, shift_out, out_sem.at[2]),
+        pltpu.make_async_copy(read_line, read_out, out_sem.at[3]),
+    ]
+    for c in ins:
+        c.start()
+    ins[0].wait()
+    outs[0].start()
+    ins[3].wait()
+    outs[1].start()
+    ins[4].wait()
+    outs[2].start()
+    ins[1].wait()
+    ins[2].wait()
+    heads = read_line.shape[1]
+    read = jnp.dot(w_buf[...], v_buf[...], preferred_element_type=jnp.float32)[:heads]
+    read_line[0] = (read * rms(read) * gain_buf[...]).astype(jnp.bfloat16)
     outs[3].start()
     for c in outs:
         c.wait()
@@ -390,16 +408,20 @@
     hbm = pl.BlockSpec(memory_space=pltpu.HBM)
     bf16 = jnp.bfloat16
     dma = lambda n: pltpu.SemaphoreType.DMA((2, n))
-    k_line, v_line, shifts = pl.pallas_call(
+    lines = pl.pallas_call(
         functools.partial(gather_kernel, nx, nz),
         out_shape=(
             jax.ShapeDtypeStruct((length, head), bf16),
             jax.ShapeDtypeStruct((length, head), bf16),
-            jax.ShapeDtypeStruct((tp,) + shift.shape[1:], bf16),
+            jax.ShapeDtypeStruct((1, 1, length), bf16),
+            jax.ShapeDtypeStruct((2 * query.shape[1], length), bf16),
         ),
-        in_specs=[hbm] * 6,
-        out_specs=(vmem, vmem, vmem),
+        in_specs=[hbm] * 8,
+        out_specs=(vmem,) * 4,
         scratch_shapes=[
+            pltpu.VMEM((tp,) + shift.shape[1:], bf16),
+            pltpu.VMEM(query.shape, bf16),
+            pltpu.VMEM((1, head), jnp.float32),
             pltpu.VMEM((CORES, rows, width), bf16),
             pltpu.VMEM((CORES, rows, width), bf16),
             pltpu.VMEM((tp // CORES, sp * depth, head), bf16),
@@ -408,14 +430,14 @@
             pltpu.VMEM((CORES, rows, head), bf16),
             pltpu.VMEM((1, width), jnp.float32),
             pltpu.VMEM((1, head), jnp.float32),
-            pltpu.SemaphoreType.DMA((6,)),
+            pltpu.SemaphoreType.DMA((8,)),
             dma(1),
             dma(3),
             dma(nz - 1),
+            dma(2 * nz),
             dma(nz),
-            dma(2 * nz),
             dma(1),
-            dma(2 * (nz - 1)),
+            dma(3 * (nz - 1)),
             dma(2 * nz),
             dma(2 * CORES),
         ],
@@ -423,7 +445,7 @@
             collective_id=0, has_side_effects=True, vmem_limit_bytes=VMEM_LIMIT
         ),
         name="gather_project",
-    )(x, gain.reshape(1, width), kw, vw, key_gain.reshape(1, head), shift)
+    )(x, gain.reshape(1, width), kw, vw, key_gain.reshape(1, head), shift, query, query_gain.reshape(1, head))
     return pl.pallas_call(
         read_kernel,
         out_shape=(
@@ -432,20 +454,21 @@
             jax.ShapeDtypeStruct((1, 1, length), bf16),
             jax.ShapeDtypeStruct(query.shape, bf16),
         ),
-        in_specs=[vmem] * 3 + [hbm] * 3,
+        in_specs=[hbm] * 5,
         out_specs=(hbm,) * 4,
         scratch_shapes=[
+            pltpu.VMEM((length, head), bf16),
+            pltpu.VMEM((length, head), bf16),
+            pltpu.VMEM((1, 1, length), bf16),
+            pltpu.VMEM((2 * query.shape[1], length), bf16),
+            pltpu.VMEM((1, head), jnp.float32),
             pltpu.VMEM(query.shape, bf16),
-            pltpu.VMEM((1, head), jnp.float32),
-            pltpu.VMEM((1, head), jnp.float32),
-            pltpu.VMEM((1, 1, length), bf16),
-            pltpu.VMEM(query.shape, bf16),
-            pltpu.SemaphoreType.DMA((3,)),
+            pltpu.SemaphoreType.DMA((5,)),
             pltpu.SemaphoreType.DMA((4,)),
         ],
         compiler_params=pltpu.CompilerParams(vmem_limit_bytes=VMEM_LIMIT),
         name="read",
-    )(k_line, v_line, shifts, query, query_gain.reshape(1, head), out_gain.reshape(1, head))
+    )(*lines, out_gain.reshape(1, head))
 
 
 def x_extent(mesh):

time: 38.6 us -> 35.7 us (0.925)
  the two profiles are of different devices: /device:TPU:10 before, /device:TPU:0 now
where the time goes in v3:
time: 35.7 us; the launch traced here: 35 us
  Pallas kernels  34.3 us (96%)
  between operations  0.64 us (2%)
    pallas_call x1, Pallas kernels, lanes_of_cores(): pl.pallas_call(functools.partial(gather_kernel, nx, nz), out_shape=(jax.S...  32.3 us
    pallas_call x1, Pallas kernels, lanes_of_cores(): pl.pallas_call(read_kernel, out_shape=(jax.ShapeDtypeStruct((1, 1, length...  2.05 us

profile of v3, /device:TPU:0, one launch (start us, length us, event | category | flops | bytes accessed | tf_op | source)
XLA Modules:
  0.0 35.0 jit_solution(8143455590079038342)
XLA Ops:
  0.6 32.3 %gather_project.1 = (bf16[1536,128]{1,0:T(8,128)(2,1)}, bf16[1536,128]{1,0:T(8,128)(2,1)}, bf16[1,1,1536]{2,1,0:T(2,128)(2,1)}, bf16[8,1536]{1,0:T(8,128)(2,1)}) custom-call(bf16[1,384,2048]{2,1,0:T(8,128)(2,1)} %x_ref.1, f32[1,2048]{1,0:T(1,128)} %bitcast.4, bf16[256,128]{1,0:T(8,128)(2,1)} %kw_ref.1, bf16[256,128]{1,0:T(8,128)(2,1)} %vw_ref.1, ...), custom_call_target="tpu_custom_call" | custom-call | tf_op jit(solution)/shard_map/gather_project/pallas_call | solution.py:411
  32.9 2.0 %read.1 = (bf16[1,1,1536,128]{3,2,1,0:T(8,128)(2,1)}, bf16[1,1,1536,128]{3,2,1,0:T(8,128)(2,1)}, bf16[1,1,1536]{2,1,0:T(2,128)(2,1)}, bf16[1,4,128]{2,1,0:T(4,128)(2,1)}) custom-call(bf16[1536,128]{1,0:T(8,128)(2,1)} %get-tuple-element.8.k_line, bf16[1536,128]{1,0:T(8,128)(2,1)} %get-tuple-element.9.v_line, ...), custom_call_target="tpu_custom_call" | custom-call | tf_op jit(solution)/shard_map/read/pallas_call | solution.py:449
